TPU v7x, 32 devices: a whole 2x2x4 slice. The times are simulated.
32 devices in a mesh: fs: 16 (over z, y, x), tp: 2 (over core).
Axes of the slice: x: 2, y: 2, z: 4, core: 2. Of those that a mesh axis runs over, the one named last changes fastest.
Arguments:
- saved_inputs: bfloat16 [12288, 2048], P('fs'), may hold values from -8 to 8
- input_cot: bfloat16 [12288, 2048], P('fs', 'tp'), may hold values from -0.0546875 to 0.0546875
- gate_cot: bfloat16 [12288, 2048], P('fs', 'tp'), may hold values from -0.0546875 to 0.0546875
- input_master: float32 [2048, 2048], P('fs', 'tp'), may hold values from -6 to 6
- gate_master: float32 [2048, 2048], P('fs', 'tp'), may hold values from -6 to 6
- input_factor: bfloat16 [2048, 256], P('fs'), may hold values from -2 to 2
- gate_factor: bfloat16 [2048, 256], P('fs'), may hold values from -2 to 2
- input_first: float32 [256, 2048], P('fs', 'tp'), may hold values from -6 to 6
- input_second: float32 [256, 2048], P('fs', 'tp'), may hold values from 0.2 to 17
- gate_first: float32 [256, 2048], P('fs', 'tp'), may hold values from -6 to 6
- gate_second: float32 [256, 2048], P('fs', 'tp'), may hold values from 0.2 to 17
Outputs:
- input_step: float32 [2048, 2048], P('fs', 'tp')
- gate_step: float32 [2048, 2048], P('fs', 'tp')
- input_first_new: float32 [256, 2048], P('fs', 'tp')
- input_second_new: float32 [256, 2048], P('fs', 'tp')
- gate_first_new: float32 [256, 2048], P('fs', 'tp')
- gate_second_new: float32 [256, 2048], P('fs', 'tp')
- input_copy: bfloat16 [2048, 2048], P(None, 'tp')
- gate_copy: bfloat16 [2048, 2048], P(None, 'tp')
All inputs are finite; a program needn't handle non-finite values.
Results may differ from a plain program's by a relative error of at most 0.0004.
Values may be sent and summed in bfloat16 or wider, within the bound.
A program may use at most 64 MiB of HBM per device.

v0:
```python
import jax
import jax.numpy as jnp
from jax import lax
from jax.sharding import PartitionSpec as P

D = 2048
W = 2048
first_decay = 0.9
second_decay = 0.9
ratio_floor = 1e-08
mean_floor = 1e-06
step_size = 0.05


def moments(low_rank, first, second):
    first_new = first_decay * first + (1.0 - first_decay) * low_rank
    second_new = second_decay * second + (1.0 - second_decay) * low_rank * low_rank
    ratio = first_new / (jnp.sqrt(second_new) + ratio_floor)
    return (first_new, second_new, ratio)


def local(
    saved_inputs,
    input_cot,
    gate_cot,
    input_master,
    gate_master,
    input_factor,
    gate_factor,
    input_first,
    input_second,
    gate_first,
    gate_second,
):
    col_width = input_cot.shape[1]
    contract = (((0,), (0,)), ((), ()))
    factor_in = input_factor.astype(jnp.float32)
    factor_gate = gate_factor.astype(jnp.float32)
    whole_in, whole_gate = (
        lax.all_gather(input_factor, "fs", axis=0, tiled=True),
        lax.all_gather(gate_factor, "fs", axis=0, tiled=True),
    )
    partial_in = lax.dot_general(
        saved_inputs, input_cot, contract, preferred_element_type=jnp.float32
    )
    partial_gate = lax.dot_general(
        saved_inputs, gate_cot, contract, preferred_element_type=jnp.float32
    )
    cols_in = whole_in.astype(jnp.float32)
    cols_gate = whole_gate.astype(jnp.float32)
    term_in = lax.dot_general(cols_in, partial_in, contract, precision=lax.Precision.HIGHEST)
    term_gate = lax.dot_general(cols_gate, partial_gate, contract, precision=lax.Precision.HIGHEST)
    summed = lax.psum_scatter(
        jnp.concatenate([term_in, term_gate], axis=1), "fs", scatter_dimension=0, tiled=True
    )
    low_in = summed[:, :col_width]
    low_gate = summed[:, col_width:]
    first_in, second_in, ratio_in = moments(low_in, input_first, input_second)
    first_gate, second_gate, ratio_gate = moments(low_gate, gate_first, gate_second)
    piece_in = lax.all_gather(ratio_in, "fs", axis=0, tiled=True)
    piece_gate = lax.all_gather(ratio_gate, "fs", axis=0, tiled=True)
    cols_in = factor_in
    cols_gate = factor_gate
    dir_in = jnp.dot(cols_in, piece_in, precision=lax.Precision.HIGHEST)
    dir_gate = jnp.dot(cols_gate, piece_gate, precision=lax.Precision.HIGHEST)
    square_in, square_gate = lax.psum(
        (jnp.sum(dir_in * dir_in), jnp.sum(dir_gate * dir_gate)), ("fs", "tp")
    )
    step_in = dir_in * lax.rsqrt(square_in / (D * W) + mean_floor)
    step_gate = dir_gate * lax.rsqrt(square_gate / (D * W) + mean_floor)
    local_in = (input_master - step_size * step_in).astype(jnp.bfloat16)
    local_gate = (gate_master - step_size * step_gate).astype(jnp.bfloat16)
    copy_in, copy_gate = (
        lax.all_gather(local_in, "fs", axis=0, tiled=True),
        lax.all_gather(local_gate, "fs", axis=0, tiled=True),
    )
    return (step_in, step_gate, first_in, second_in, first_gate, second_gate, copy_in, copy_gate)


def solution(mesh):
    return jax.shard_map(
        local,
        mesh=mesh,
        in_specs=(
            P("fs", None),
            P("fs", "tp"),
            P("fs", "tp"),
            P("fs", "tp"),
            P("fs", "tp"),
            P("fs", None),
            P("fs", None),
            P("fs", "tp"),
            P("fs", "tp"),
            P("fs", "tp"),
            P("fs", "tp"),
        ),
        out_specs=(
            P("fs", "tp"),
            P("fs", "tp"),
            P("fs", "tp"),
            P("fs", "tp"),
            P("fs", "tp"),
            P("fs", "tp"),
            P(None, "tp"),
            P(None, "tp"),
        ),
        check_vma=False,
    )
```

profile of v0, /device:TPU:0, one launch (start us, length us, event | category | flops | bytes accessed | tf_op | source)
XLA Modules:
  0.0 569.3 jit_solution(10387800890137530023)
XLA Ops:
  7.2 0.0 copy-start
  7.2 0.0 all-gather.7.cloned.1.call-start
  7.2 0.7 all-gather.7.cloned.1.call-update
  7.9 0.0 all-gather.9.cloned.1.call-start
  8.0 0.7 all-gather.9.cloned.1.call-update
  8.7 0.0 reduce-scatter.4.cloned.1.call-start
  8.7 0.3 copy-done
  9.1 0.0 copy-start.8
  9.1 7.2 %fusion.4 = f32[2048,1024]{1,0:T(8,128)} fusion(bf16[768,2048]{1,0:T(8,128)(2,1)S(1)} %copy-done, bf16[768,1024]{1,0:T(8,128)(2,1)} %param.12), kind=kOutput, calls=%fused_computation.17 | convolution fusion | flops 3221225472 | bytes 13107200 | tf_op jit(solution)/shard_map/dot_general | solution.py:43
  16.2 0.0 copy-done.8
  16.2 5.7 %fusion.5 = f32[2048,1024]{1,0:T(8,128)} fusion(bf16[768,2048]{1,0:T(8,128)(2,1)S(1)} %copy-done, bf16[768,1024]{1,0:T(8,128)(2,1)S(1)} %copy-done.8), kind=kOutput, calls=%fused_computation.18 | convolution fusion | flops 3221225472 | bytes 13107200 | tf_op jit(solution)/shard_map/dot_general | solution.py:46
  21.9 46.7 %all-gather.7.cloned.1.call-done = bf16[2048,256]{1,0:T(8,128)(2,1)} async-done(((bf16[128,256]{1,0:T(8,128)(2,1)}), bf16[2048,256]{1,0:T(8,128)(2,1)}) %all-gather.7.cloned.1.call-update) | async-done | bytes 1048592 | tf_op jit(solution)/shard_map/all_gather | solution.py:40
  68.6 11.2 %convolution_bitcast_fusion.1 = f32[256,1024]{0,1:T(8,128)} fusion(f32[2048,1024]{1,0:T(8,128)} %fusion.4, bf16[2048,256]{1,0:T(8,128)(2,1)} %all-gather.7.cloned.1.call-done), kind=kOutput, calls=%fused_computation.2 | convolution fusion | flops 6442450944 | bytes 10485760 | tf_op jit(solution)/shard_map/dot_general | solution.py:51
  79.8 45.5 %all-gather.9.cloned.1.call-done = bf16[2048,256]{1,0:T(8,128)(2,1)} async-done(((bf16[128,256]{1,0:T(8,128)(2,1)}), bf16[2048,256]{1,0:T(8,128)(2,1)}) %all-gather.9.cloned.1.call-update) | async-done | bytes 1048592 | tf_op jit(solution)/shard_map/all_gather | solution.py:41
  125.3 0.0 copy-start.1
  125.3 9.5 %convolution_bitcast_fusion = f32[256,1024]{0,1:T(8,128)S(1)} fusion(f32[2048,1024]{1,0:T(8,128)} %fusion.5, bf16[2048,256]{1,0:T(8,128)(2,1)} %all-gather.9.cloned.1.call-done), kind=kOutput, calls=%fused_computation.1 | convolution fusion | flops 6442450944 | bytes 10485760 | tf_op jit(solution)/shard_map/dot_general | solution.py:52
  134.8 0.0 copy-done.1
  134.8 1.5 pad_maximum_fusion
  136.2 0.0 copy-start.4
  136.2 0.0 copy-start.5
  136.2 0.0 copy-start.6
  136.2 0.0 copy-start.7
  136.2 0.0 copy-start.2
  136.3 2.9 copy.65
  139.2 0.0 copy-start.3
  139.2 0.0 reduce-scatter.4.cloned.1.call-update
  139.2 0.0 all-gather.13.cloned.1.call-start
  139.3 80.6 %reduce-scatter.4.cloned.1.call-done = f32[16,2048]{1,0:T(8,128)} async-done(((f32[256,2048]{1,0:T(8,128)}), f32[16,2048]{1,0:T(8,128)}) %reduce-scatter.4.cloned.1.call-update) | async-done | bytes 131088 | tf_op jit(solution)/shard_map/reduce_scatter | solution.py:53
  219.9 0.0 copy-done.4
  219.9 0.0 copy-done.5
  219.9 0.0 copy-done.6
  219.9 0.0 copy-done.7
  219.9 1.6 add_divide_fusion
  221.5 0.0 all-gather.13.cloned.1.call-update
  221.5 0.0 all-gather.11.cloned.1.call-start
  221.6 0.5 all-gather.11.cloned.1.call-update
  222.1 0.0 all-gather.15.cloned.1.call-start
  222.2 2.0 copy.59
  224.2 50.4 %all-gather.13.cloned.1.call-done = f32[256,1024]{1,0:T(8,128)} async-done(((f32[16,1024]{1,0:T(8,128)}), f32[256,1024]{1,0:T(8,128)}) %all-gather.13.cloned.1.call-update) | async-done | bytes 1048592 | tf_op jit(solution)/shard_map/all_gather | solution.py:61
  274.6 0.0 copy-done.2
  274.6 3.7 multiply_reduce_fusion
  278.3 53.4 %all-gather.11.cloned.1.call-done = f32[256,1024]{1,0:T(8,128)} async-done(((f32[16,1024]{1,0:T(8,128)}), f32[256,1024]{1,0:T(8,128)}) %all-gather.11.cloned.1.call-update) | async-done | bytes 1048592 | tf_op jit(solution)/shard_map/all_gather | solution.py:60
  331.7 0.0 copy-done.3
  331.7 3.6 multiply_reduce_fusion.1
  335.4 38.6 %all-reduce = (f32[]{:T(128)}, f32[]{:T(128)}) all-reduce(f32[]{:T(128)} %get-tuple-element.47, f32[]{:T(128)} %get-tuple-element.49), channel_id=1, replica_groups=mesh['fs'=16,'tp'=2] {'fs','tp'}, use_global_device_ids=true, to_apply=%region_2.0 | all-reduce | flops 2 | bytes 16 | tf_op jit(solution)/shard_map/psum | solution.py:66
  374.7 2.2 subtract_convert_fusion.1
  376.8 0.0 all-gather.15.cloned.1.call-update
  376.9 0.0 all-gather.17.cloned.1.call-start
  376.9 2.0 copy.60
  379.7 2.2 subtract_convert_fusion
  381.8 0.0 all-gather.17.cloned.1.call-update
  381.9 2.0 copy.61
  383.9 2.0 copy.62
  385.9 80.5 %all-gather.15.cloned.1.call-done = bf16[2048,1024]{0,1:T(8,128)(2,1)} async-done(((bf16[128,1024]{0,1:T(8,128)(2,1)}), bf16[2048,1024]{0,1:T(8,128)(2,1)}) %all-gather.15.cloned.1.call-update) | async-done | bytes 4194320 | tf_op jit(solution)/shard_map/all_gather | solution.py:74
  466.4 6.4 %copy.63 = bf16[2048,1024]{1,0:T(8,128)(2,1)} copy(bf16[2048,1024]{0,1:T(8,128)(2,1)} %all-gather.15.cloned.1.call-done) | data formatting | bytes 8388608
  472.8 83.2 %all-gather.17.cloned.1.call-done = bf16[2048,1024]{0,1:T(8,128)(2,1)} async-done(((bf16[128,1024]{0,1:T(8,128)(2,1)}), bf16[2048,1024]{0,1:T(8,128)(2,1)}) %all-gather.17.cloned.1.call-update) | async-done | bytes 4194320 | tf_op jit(solution)/shard_map/all_gather | solution.py:75
  556.0 6.4 %copy.64 = bf16[2048,1024]{1,0:T(8,128)(2,1)} copy(bf16[2048,1024]{0,1:T(8,128)(2,1)} %all-gather.17.cloned.1.call-done) | data formatting | bytes 8388608
Async XLA Ops:
  7.2 1.9 copy-start
  7.2 61.4 %all-gather.7.cloned.1.call-start = ((), (), s32[]{:S(2)}) async-start(), calls=%async_computation.1 | async-start | bytes 1114112 | tf_op jit(solution)/shard_map/all_gather | solution.py:40
  7.9 117.4 %all-gather.9.cloned.1.call-start = ((), (), s32[]{:S(2)}) async-start(), calls=%async_computation.2 | async-start | bytes 1114112 | tf_op jit(solution)/shard_map/all_gather | solution.py:41
  8.7 211.2 %reduce-scatter.4.cloned.1.call-start = ((), (), s32[]{:S(2)}) async-start(), calls=%async_computation.7 | async-start | bytes 2228224 | tf_op jit(solution)/shard_map/reduce_scatter | solution.py:53
  9.1 7.2 %copy-start.8 = (bf16[768,1024]{1,0:T(8,128)(2,1)S(1)}, bf16[768,1024]{1,0:T(8,128)(2,1)}, u32[]{:S(2)}) copy-start(bf16[768,1024]{1,0:T(8,128)(2,1)} %param.13) | copy-start | bytes 4718596
  125.3 9.5 %copy-start.1 = (f32[256,1024]{0,1:T(8,128)S(1)}, f32[256,1024]{0,1:T(8,128)}, u32[]{:S(2)}) copy-start(f32[256,1024]{0,1:T(8,128)} %convolution_bitcast_fusion.1) | copy-start | bytes 3145732
  136.2 83.6 %copy-start.4 = (f32[16,1024]{1,0:T(8,128)S(1)}, f32[16,1024]{1,0:T(8,128)}, u32[]{:S(2)}) copy-start(f32[16,1024]{1,0:T(8,128)} %param.21) | copy-start | bytes 196612
  136.2 83.6 %copy-start.5 = (f32[16,1024]{1,0:T(8,128)S(1)}, f32[16,1024]{1,0:T(8,128)}, u32[]{:S(2)}) copy-start(f32[16,1024]{1,0:T(8,128)} %param.20) | copy-start | bytes 196612
  136.2 83.6 %copy-start.6 = (f32[16,1024]{1,0:T(8,128)S(1)}, f32[16,1024]{1,0:T(8,128)}, u32[]{:S(2)}) copy-start(f32[16,1024]{1,0:T(8,128)} %param.19) | copy-start | bytes 196612
  136.2 83.6 %copy-start.7 = (f32[16,1024]{1,0:T(8,128)S(1)}, f32[16,1024]{1,0:T(8,128)}, u32[]{:S(2)}) copy-start(f32[16,1024]{1,0:T(8,128)} %param.18) | copy-start | bytes 196612
  136.2 138.3 %copy-start.2 = (bf16[128,256]{1,0:T(8,128)(2,1)S(1)}, bf16[128,256]{1,0:T(8,128)(2,1)}, u32[]{:S(2)}) copy-start(bf16[128,256]{1,0:T(8,128)(2,1)} %param.17) | copy-start | bytes 196612
  139.2 192.5 %copy-start.3 = (bf16[128,256]{1,0:T(8,128)(2,1)S(1)}, bf16[128,256]{1,0:T(8,128)(2,1)}, u32[]{:S(2)}) copy-start(bf16[128,256]{1,0:T(8,128)(2,1)} %param.16) | copy-start | bytes 196612
  139.2 135.4 %all-gather.13.cloned.1.call-start = ((), (), s32[]{:S(2)}) async-start(), calls=%async_computation.4 | async-start | bytes 1114112 | tf_op jit(solution)/shard_map/all_gather | solution.py:61
  221.5 110.2 %all-gather.11.cloned.1.call-start = ((), (), s32[]{:S(2)}) async-start(), calls=%async_computation.3 | async-start | bytes 1114112 | tf_op jit(solution)/shard_map/all_gather | solution.py:60
  222.1 244.3 %all-gather.15.cloned.1.call-start = ((), (), s32[]{:S(2)}) async-start(), calls=%async_computation.5 | async-start | bytes 4456448 | tf_op jit(solution)/shard_map/all_gather | solution.py:74
  376.9 179.2 %all-gather.17.cloned.1.call-start = ((), (), s32[]{:S(2)}) async-start(), calls=%async_computation.6 | async-start | bytes 4456448 | tf_op jit(solution)/shard_map/all_gather | solution.py:75
Sparse Core Ops, SparseCore 0:
  10.7 57.7 all-gather.6
  71.3 53.9 all-gather.8
  139.3 80.4 reduce-scatter.3
  223.0 51.4 all-gather.12
  277.8 53.9 all-gather.10
  377.0 89.3 all-gather.14
  469.1 86.8 all-gather.16
where the time goes:
time: 570 us; the launch traced here: 569 us
  waiting for transfers between devices  442 us (78%)
  matrix products  40.9 us (7%)
  blocking collectives  38.6 us (7%)
  local copies, waits for them, and re-layouts  24.2 us (4%)
  between operations  15.6 us (3%)
  other arithmetic  7.42 us (1%)
    all_gather x1, waiting for transfers between devices, local(): lax.all_gather(local_gate, 'fs', axis=0, tiled=True)  83.2 us
    reduce_scatter x1, waiting for transfers between devices, local(): lax.psum_scatter(jnp.concatenate([term_in, term_gate], axis=1), 'fs', sca...  80.6 us
    all_gather x1, waiting for transfers between devices, local(): lax.all_gather(local_in, 'fs', axis=0, tiled=True)  80.5 us
    all_gather x1, waiting for transfers between devices, local(): piece_in = lax.all_gather(ratio_in, 'fs', axis=0, tiled=True)  53.4 us
    all_gather x1, waiting for transfers between devices, local(): piece_gate = lax.all_gather(ratio_gate, 'fs', axis=0, tiled=True)  50.4 us
    all_gather x1, waiting for transfers between devices, local(): lax.all_gather(input_factor, 'fs', axis=0, tiled=True)  46.7 us
    all_gather x1, waiting for transfers between devices, local(): lax.all_gather(gate_factor, 'fs', axis=0, tiled=True)  45.5 us
    psum x1, blocking collectives, local(): lax.psum((jnp.sum(dir_in * dir_in), jnp.sum(dir_gate * dir_gate)), ('fs',...  38.6 us
  transfers between devices with their start and end apart: 7, of which 7 were waited for; matrix products, arithmetic and copies ran while one was open for 8% of the time, Pallas kernels for 0%

commit v1 on v0

--- a/solution.py
+++ b/solution.py
@@ -10,6 +10,16 @@
 ratio_floor = 1e-08
 mean_floor = 1e-06
 step_size = 0.05
+
+
+def around_the_ring(array, mesh_axis, dim):
+    size = lax.axis_size(mesh_axis)
+    current, blocks = (array, [array])
+    for _ in range(size - 1):
+        current = lax.ppermute(current, mesh_axis, [(i, (i + 1) % size) for i in range(size)])
+        blocks.insert(0, current)
+    line = jnp.concatenate(blocks, axis=dim)
+    return jnp.roll(line, (lax.axis_index(mesh_axis) + 1) * array.shape[dim], axis=dim)
 
 
 def moments(low_rank, first, second):
@@ -58,7 +68,7 @@
     first_in, second_in, ratio_in = moments(low_in, input_first, input_second)
     first_gate, second_gate, ratio_gate = moments(low_gate, gate_first, gate_second)
     piece_in = lax.all_gather(ratio_in, "fs", axis=0, tiled=True)
-    piece_gate = lax.all_gather(ratio_gate, "fs", axis=0, tiled=True)
+    piece_gate = around_the_ring(ratio_gate, "fs", 0)
     cols_in = factor_in
     cols_gate = factor_gate
     dir_in = jnp.dot(cols_in, piece_in, precision=lax.Precision.HIGHEST)

time: 570 us -> 635 us (1.11)
  waiting for transfers between devices: 442 us -> 491 us
  local copies, waits for them, and re-layouts: 24.2 us -> 41.2 us
    ppermute x0 -> x15, waiting for transfers between devices: none -> 117 us  [around_the_ring(): lax.ppermute(current, mesh_axis, [(i, (i + 1) % size) for i in range(size)])]
    all_gather x1 -> x0, waiting for transfers between devices: 50.4 us -> none  [local(): piece_gate = lax.all_gather(ratio_gate, 'fs', axis=0, tiled=True)]
    all_gather x1, waiting for transfers between devices: 53.4 us -> 35.9 us  [local(): piece_in = lax.all_gather(ratio_in, 'fs', axis=0, tiled=True)]
    unnamed x25 -> x94, local copies, waits for them, and re-layouts: 24.2 us -> 41.2 us
  transfers between devices with their start and end apart: 7 -> 21, of which waited for: 7 -> 21; matrix products, arithmetic and copies ran while one was open for 8% -> 9% of each run, Pallas kernels for 0% -> 0%
where the time goes in v1:
time: 635 us; the launch traced here: 634 us
  waiting for transfers between devices  491 us (77%)
  local copies, waits for them, and re-layouts  41.2 us (6%)
  matrix products  39.6 us (6%)
  blocking collectives  38.6 us (6%)
  between operations  15.9 us (3%)
  other arithmetic  7.41 us (1%)
    ppermute x15, waiting for transfers between devices, around_the_ring(): lax.ppermute(current, mesh_axis, [(i, (i + 1) % size) for i in range(size)])  117 us
    all_gather x1, waiting for transfers between devices, local(): lax.all_gather(local_gate, 'fs', axis=0, tiled=True)  83.1 us
    reduce_scatter x1, waiting for transfers between devices, local(): lax.psum_scatter(jnp.concatenate([term_in, term_gate], axis=1), 'fs', sca...  80.6 us
    all_gather x1, waiting for transfers between devices, local(): lax.all_gather(local_in, 'fs', axis=0, tiled=True)  80.5 us
    all_gather x1, waiting for transfers between devices, local(): lax.all_gather(input_factor, 'fs', axis=0, tiled=True)  46.7 us
    all_gather x1, waiting for transfers between devices, local(): lax.all_gather(gate_factor, 'fs', axis=0, tiled=True)  45.5 us
    unnamed x94, local copies, waits for them, and re-layouts  41.2 us
    psum x1, blocking collectives, local(): lax.psum((jnp.sum(dir_in * dir_in), jnp.sum(dir_gate * dir_gate)), ('fs',...  38.6 us
  transfers between devices with their start and end apart: 21, of which 21 were waited for; matrix products, arithmetic and copies ran while one was open for 9% of the time, Pallas kernels for 0%

profile of v1, /device:TPU:0, one launch (start us, length us, event | category | flops | bytes accessed | tf_op | source)
XLA Modules:
  0.0 633.6 jit_solution(2017384833539791759)
XLA Ops:
  7.2 0.7 all-gather.6.cloned.1.call-update
  8.0 0.7 all-gather.8.cloned.1.call-update
  8.7 0.3 copy-done
  9.1 7.1 %fusion.7 = f32[2048,1024]{1,0:T(8,128)} fusion(bf16[768,2048]{1,0:T(8,128)(2,1)S(1)} %copy-done, bf16[768,1024]{1,0:T(8,128)(2,1)} %param.12), kind=kOutput, calls=%fused_computation.52 | convolution fusion | flops 3221225472 | bytes 13107200 | tf_op jit(solution)/shard_map/dot_general | solution.py:53
  16.2 5.7 fusion.8
  21.9 46.7 %all-gather.6.cloned.1.call-done = bf16[2048,256]{1,0:T(8,128)(2,1)} async-done(((bf16[128,256]{1,0:T(8,128)(2,1)}), bf16[2048,256]{1,0:T(8,128)(2,1)}) %all-gather.6.cloned.1.call-update) | async-done | bytes 1048592 | tf_op jit(solution)/shard_map/all_gather | solution.py:50
  68.6 11.2 %convolution_bitcast_fusion.1 = f32[256,1024]{0,1:T(8,128)} fusion(f32[2048,1024]{1,0:T(8,128)} %fusion.7, bf16[2048,256]{1,0:T(8,128)(2,1)} %all-gather.6.cloned.1.call-done), kind=kOutput, calls=%fused_computation.2 | convolution fusion | flops 6442450944 | bytes 10485760 | tf_op jit(solution)/shard_map/dot_general | solution.py:61
  79.8 45.5 %all-gather.8.cloned.1.call-done = bf16[2048,256]{1,0:T(8,128)(2,1)} async-done(((bf16[128,256]{1,0:T(8,128)(2,1)}), bf16[2048,256]{1,0:T(8,128)(2,1)}) %all-gather.8.cloned.1.call-update) | async-done | bytes 1048592 | tf_op jit(solution)/shard_map/all_gather | solution.py:51
  125.3 9.5 %convolution_bitcast_fusion = f32[256,1024]{0,1:T(8,128)S(1)} fusion(f32[2048,1024]{1,0:T(8,128)} %fusion.8, bf16[2048,256]{1,0:T(8,128)(2,1)} %all-gather.8.cloned.1.call-done), kind=kOutput, calls=%fused_computation.1 | convolution fusion | flops 6442450944 | bytes 10485760 | tf_op jit(solution)/shard_map/dot_general | solution.py:62
  134.8 1.5 pad_maximum_fusion
  136.2 2.9 copy.64
  139.2 80.6 %reduce-scatter.4.cloned.1.call-done = f32[16,2048]{1,0:T(8,128)} async-done(((f32[256,2048]{1,0:T(8,128)}), f32[16,2048]{1,0:T(8,128)}) %reduce-scatter.4.cloned.1.call-update) | async-done | bytes 131088 | tf_op jit(solution)/shard_map/reduce_scatter | solution.py:63
  219.8 1.6 add_divide_fusion
  221.4 7.9 %collective-permute-done = f32[16,1024]{1,0:T(8,128)S(1)} collective-permute-done((f32[16,1024]{1,0:T(8,128)S(1)}, f32[16,1024]{1,0:T(8,128)S(1)}, u32[]{:S(2)}, u32[]{:S(2)}) %collective-permute-start) | collective-permute-done | bytes 65568 | tf_op jit(solution)/shard_map/ppermute | solution.py:19
  229.3 8.5 %collective-permute-done.1 = f32[16,1024]{1,0:T(8,128)S(1)} collective-permute-done((f32[16,1024]{1,0:T(8,128)S(1)}, f32[16,1024]{1,0:T(8,128)S(1)}, u32[]{:S(2)}, u32[]{:S(2)}) %collective-permute-start.1) | collective-permute-done | bytes 65568 | tf_op jit(solution)/shard_map/ppermute | solution.py:19
  237.8 7.9 %collective-permute-done.2 = f32[16,1024]{1,0:T(8,128)S(1)} collective-permute-done((f32[16,1024]{1,0:T(8,128)S(1)}, f32[16,1024]{1,0:T(8,128)S(1)}, u32[]{:S(2)}, u32[]{:S(2)}) %collective-permute-start.2) | collective-permute-done | bytes 65568 | tf_op jit(solution)/shard_map/ppermute | solution.py:19
  245.6 7.9 %collective-permute-done.3 = f32[16,1024]{1,0:T(8,128)S(1)} collective-permute-done((f32[16,1024]{1,0:T(8,128)S(1)}, f32[16,1024]{1,0:T(8,128)S(1)}, u32[]{:S(2)}, u32[]{:S(2)}) %collective-permute-start.3) | collective-permute-done | bytes 65568 | tf_op jit(solution)/shard_map/ppermute | solution.py:19
  253.5 7.9 %collective-permute-done.4 = f32[16,1024]{1,0:T(8,128)S(1)} collective-permute-done((f32[16,1024]{1,0:T(8,128)S(1)}, f32[16,1024]{1,0:T(8,128)S(1)}, u32[]{:S(2)}, u32[]{:S(2)}) %collective-permute-start.4) | collective-permute-done | bytes 65568 | tf_op jit(solution)/shard_map/ppermute | solution.py:19
  261.4 7.9 %collective-permute-done.5 = f32[16,1024]{1,0:T(8,128)S(1)} collective-permute-done((f32[16,1024]{1,0:T(8,128)S(1)}, f32[16,1024]{1,0:T(8,128)S(1)}, u32[]{:S(2)}, u32[]{:S(2)}) %collective-permute-start.5) | collective-permute-done | bytes 65568 | tf_op jit(solution)/shard_map/ppermute | solution.py:19
  269.2 0.6 copy-done.7
  269.8 7.9 %collective-permute-done.6 = f32[16,1024]{1,0:T(8,128)S(1)} collective-permute-done((f32[16,1024]{1,0:T(8,128)S(1)}, f32[16,1024]{1,0:T(8,128)S(1)}, u32[]{:S(2)}, u32[]{:S(2)}) %collective-permute-start.6) | collective-permute-done | bytes 65568 | tf_op jit(solution)/shard_map/ppermute | solution.py:19
  277.7 0.6 copy-done.9
  278.3 7.9 %collective-permute-done.7 = f32[16,1024]{1,0:T(8,128)S(1)} collective-permute-done((f32[16,1024]{1,0:T(8,128)S(1)}, f32[16,1024]{1,0:T(8,128)S(1)}, u32[]{:S(2)}, u32[]{:S(2)}) %collective-permute-start.7) | collective-permute-done | bytes 65568 | tf_op jit(solution)/shard_map/ppermute | solution.py:19
  286.2 0.6 copy-done.11
  286.8 7.9 %collective-permute-done.8 = f32[16,1024]{1,0:T(8,128)S(1)} collective-permute-done((f32[16,1024]{1,0:T(8,128)S(1)}, f32[16,1024]{1,0:T(8,128)S(1)}, u32[]{:S(2)}, u32[]{:S(2)}) %collective-permute-start.8) | collective-permute-done | bytes 65568 | tf_op jit(solution)/shard_map/ppermute | solution.py:19
  294.6 0.6 copy-done.13
  295.3 8.2 %collective-permute-done.9 = f32[16,1024]{1,0:T(8,128)S(1)} collective-permute-done((f32[16,1024]{1,0:T(8,128)S(1)}, f32[16,1024]{1,0:T(8,128)S(1)}, u32[]{:S(2)}, u32[]{:S(2)}) %collective-permute-start.9) | collective-permute-done | bytes 65568 | tf_op jit(solution)/shard_map/ppermute | solution.py:19
  303.5 0.6 copy-done.15
  304.1 7.9 %collective-permute-done.10 = f32[16,1024]{1,0:T(8,128)S(1)} collective-permute-done((f32[16,1024]{1,0:T(8,128)S(1)}, f32[16,1024]{1,0:T(8,128)S(1)}, u32[]{:S(2)}, u32[]{:S(2)}) %collective-permute-start.10) | collective-permute-done | bytes 65568 | tf_op jit(solution)/shard_map/ppermute | solution.py:19
  312.0 0.6 copy-done.17
  312.6 7.9 %collective-permute-done.11 = f32[16,1024]{1,0:T(8,128)S(1)} collective-permute-done((f32[16,1024]{1,0:T(8,128)S(1)}, f32[16,1024]{1,0:T(8,128)S(1)}, u32[]{:S(2)}, u32[]{:S(2)}) %collective-permute-start.11) | collective-permute-done | bytes 65568 | tf_op jit(solution)/shard_map/ppermute | solution.py:19
  320.5 0.6 copy-done.19
  321.1 7.9 %collective-permute-done.12 = f32[16,1024]{1,0:T(8,128)S(1)} collective-permute-done((f32[16,1024]{1,0:T(8,128)S(1)}, f32[16,1024]{1,0:T(8,128)S(1)}, u32[]{:S(2)}, u32[]{:S(2)}) %collective-permute-start.12) | collective-permute-done | bytes 65568 | tf_op jit(solution)/shard_map/ppermute | solution.py:19
  329.0 0.6 copy-done.21
  329.6 8.0 %collective-permute-done.13 = f32[16,1024]{1,0:T(8,128)} collective-permute-done((f32[16,1024]{1,0:T(8,128)S(1)}, f32[16,1024]{1,0:T(8,128)}, u32[]{:S(2)}, u32[]{:S(2)}) %collective-permute-start.13) | collective-permute-done | bytes 65568 | tf_op jit(solution)/shard_map/ppermute | solution.py:19
  337.6 2.0 copy.58
  339.8 6.0 collective-permute-done.14
  345.7 0.8 constant_dynamic-update-slice_fusion.31
  346.6 0.8 constant_dynamic-update-slice_fusion.30
  347.4 0.8 constant_dynamic-update-slice_fusion.29
  348.3 0.8 constant_dynamic-update-slice_fusion.28
  349.1 0.8 constant_dynamic-update-slice_fusion.27
  350.0 0.8 constant_dynamic-update-slice_fusion.26
  350.8 0.8 constant_dynamic-update-slice_fusion.25
  351.7 0.8 constant_dynamic-update-slice_fusion.24
  352.5 0.8 constant_dynamic-update-slice_fusion.23
  353.3 0.8 constant_dynamic-update-slice_fusion.22
  354.2 0.8 constant_dynamic-update-slice_fusion.21
  355.1 0.8 constant_dynamic-update-slice_fusion.15
  356.0 0.8 constant_dynamic-update-slice_fusion.14
  357.0 0.8 constant_dynamic-update-slice_fusion.4
  357.9 2.4 multiply_reduce_fusion
  360.4 35.9 %all-gather.10.cloned.1.call-done = f32[256,1024]{1,0:T(8,128)} async-done(((f32[16,1024]{1,0:T(8,128)}), f32[256,1024]{1,0:T(8,128)}) %all-gather.10.cloned.1.call-update) | async-done | bytes 1048592 | tf_op jit(solution)/shard_map/all_gather | solution.py:70
  396.3 3.6 multiply_reduce_fusion.1
  399.9 38.6 %all-reduce = (f32[]{:T(128)}, f32[]{:T(128)}) all-reduce(f32[]{:T(128)} %get-tuple-element.47, f32[]{:T(128)} %get-tuple-element.49), channel_id=1, replica_groups=mesh['fs'=16,'tp'=2] {'fs','tp'}, use_global_device_ids=true, to_apply=%region_2.3 | all-reduce | flops 2 | bytes 16 | tf_op jit(solution)/shard_map/psum | solution.py:76
  439.2 2.2 subtract_convert_fusion.1
  441.4 2.0 copy.59
  444.1 2.2 subtract_convert_fusion
  446.3 2.0 copy.60
  448.4 2.0 copy.61
  450.4 80.5 %all-gather.12.cloned.1.call-done = bf16[2048,1024]{0,1:T(8,128)(2,1)} async-done(((bf16[128,1024]{0,1:T(8,128)(2,1)}), bf16[2048,1024]{0,1:T(8,128)(2,1)}) %all-gather.12.cloned.1.call-update) | async-done | bytes 4194320 | tf_op jit(solution)/shard_map/all_gather | solution.py:84
  530.9 6.4 %copy.62 = bf16[2048,1024]{1,0:T(8,128)(2,1)} copy(bf16[2048,1024]{0,1:T(8,128)(2,1)} %all-gather.12.cloned.1.call-done) | data formatting | bytes 8388608
  537.3 83.1 %all-gather.14.cloned.1.call-done = bf16[2048,1024]{0,1:T(8,128)(2,1)} async-done(((bf16[128,1024]{0,1:T(8,128)(2,1)}), bf16[2048,1024]{0,1:T(8,128)(2,1)}) %all-gather.14.cloned.1.call-update) | async-done | bytes 4194320 | tf_op jit(solution)/shard_map/all_gather | solution.py:85
  620.4 6.4 %copy.63 = bf16[2048,1024]{1,0:T(8,128)(2,1)} copy(bf16[2048,1024]{0,1:T(8,128)(2,1)} %all-gather.14.cloned.1.call-done) | data formatting | bytes 8388608
  (90 shorter events, 0.6 us)
Async XLA Ops:
  7.2 1.9 copy-start
  7.2 61.4 %all-gather.6.cloned.1.call-start = ((), (), s32[]{:S(2)}) async-start(), calls=%async_computation.1 | async-start | bytes 1114112 | tf_op jit(solution)/shard_map/all_gather | solution.py:50
  7.9 117.4 %all-gather.8.cloned.1.call-start = ((), (), s32[]{:S(2)}) async-start(), calls=%async_computation.2 | async-start | bytes 1114112 | tf_op jit(solution)/shard_map/all_gather | solution.py:51
  8.7 211.1 %reduce-scatter.4.cloned.1.call-start = ((), (), s32[]{:S(2)}) async-start(), calls=%async_computation.6 | async-start | bytes 2228224 | tf_op jit(solution)/shard_map/reduce_scatter | solution.py:63
  9.1 7.2 %copy-start.27 = (bf16[768,1024]{1,0:T(8,128)(2,1)S(1)}, bf16[768,1024]{1,0:T(8,128)(2,1)}, u32[]{:S(2)}) copy-start(bf16[768,1024]{1,0:T(8,128)(2,1)} %param.13) | copy-start | bytes 4718596
  125.3 9.5 %copy-start.1 = (f32[256,1024]{0,1:T(8,128)S(1)}, f32[256,1024]{0,1:T(8,128)}, u32[]{:S(2)}) copy-start(f32[256,1024]{0,1:T(8,128)} %convolution_bitcast_fusion.1) | copy-start | bytes 3145732
  139.1 80.7 %copy-start.23 = (f32[16,1024]{1,0:T(8,128)S(1)}, f32[16,1024]{1,0:T(8,128)}, u32[]{:S(2)}) copy-start(f32[16,1024]{1,0:T(8,128)} %param.21) | copy-start | bytes 196612
  139.1 80.7 %copy-start.24 = (f32[16,1024]{1,0:T(8,128)S(1)}, f32[16,1024]{1,0:T(8,128)}, u32[]{:S(2)}) copy-start(f32[16,1024]{1,0:T(8,128)} %param.20) | copy-start | bytes 196612
  139.1 80.7 %copy-start.25 = (f32[16,1024]{1,0:T(8,128)S(1)}, f32[16,1024]{1,0:T(8,128)}, u32[]{:S(2)}) copy-start(f32[16,1024]{1,0:T(8,128)} %param.19) | copy-start | bytes 196612
  139.1 80.7 %copy-start.26 = (f32[16,1024]{1,0:T(8,128)S(1)}, f32[16,1024]{1,0:T(8,128)}, u32[]{:S(2)}) copy-start(f32[16,1024]{1,0:T(8,128)} %param.18) | copy-start | bytes 196612
  139.2 257.1 %all-gather.10.cloned.1.call-start = ((), (), s32[]{:S(2)}) async-start(), calls=%async_computation.3 | async-start | bytes 1114112 | tf_op jit(solution)/shard_map/all_gather | solution.py:70
  221.4 7.9 %collective-permute-start = (f32[16,1024]{1,0:T(8,128)S(1)}, f32[16,1024]{1,0:T(8,128)S(1)}, u32[]{:S(2)}, u32[]{:S(2)}) collective-permute-start(f32[16,1024]{1,0:T(8,128)S(1)} %get-tuple-element.38), channel_id=1, source_target_pairs={{0,2},{2,4},{4,6},{6,8},{8,10},{10,12},{12,14},{14,16},{16,18},{18... | collective-permute-start | bytes 196616 | tf_op jit(solution)/shard_map/ppermute | solution.py:19
  229.3 8.5 %collective-permute-start.1 = (f32[16,1024]{1,0:T(8,128)S(1)}, f32[16,1024]{1,0:T(8,128)S(1)}, u32[]{:S(2)}, u32[]{:S(2)}) collective-permute-start(f32[16,1024]{1,0:T(8,128)S(1)} %collective-permute-done), channel_id=1, source_target_pairs={{0,2},{2,4},{4,6},{6,8},{8,10},{10,12},{12,14},{14,16},{16,18},{18... | collective-permute-start | bytes 196616 | tf_op jit(solution)/shard_map/ppermute | solution.py:19
  237.8 7.9 %collective-permute-start.2 = (f32[16,1024]{1,0:T(8,128)S(1)}, f32[16,1024]{1,0:T(8,128)S(1)}, u32[]{:S(2)}, u32[]{:S(2)}) collective-permute-start(f32[16,1024]{1,0:T(8,128)S(1)} %collective-permute-done.1), channel_id=1, source_target_pairs={{0,2},{2,4},{4,6},{6,8},{8,10},{10,12},{12,14},{14,16},{16,18},{18... | collective-permute-start | bytes 196616 | tf_op jit(solution)/shard_map/ppermute | solution.py:19
  245.6 7.9 %collective-permute-start.3 = (f32[16,1024]{1,0:T(8,128)S(1)}, f32[16,1024]{1,0:T(8,128)S(1)}, u32[]{:S(2)}, u32[]{:S(2)}) collective-permute-start(f32[16,1024]{1,0:T(8,128)S(1)} %collective-permute-done.2), channel_id=1, source_target_pairs={{0,2},{2,4},{4,6},{6,8},{8,10},{10,12},{12,14},{14,16},{16,18},{18... | collective-permute-start | bytes 196616 | tf_op jit(solution)/shard_map/ppermute | solution.py:19
  253.5 101.6 %copy-start.4 = (f32[16,1024]{1,0:T(8,128)}, f32[16,1024]{1,0:T(8,128)S(1)}, u32[]{:S(2)}) copy-start(f32[16,1024]{1,0:T(8,128)S(1)} %collective-permute-done.3) | copy-start | bytes 196612
  253.5 7.9 %collective-permute-start.4 = (f32[16,1024]{1,0:T(8,128)S(1)}, f32[16,1024]{1,0:T(8,128)S(1)}, u32[]{:S(2)}, u32[]{:S(2)}) collective-permute-start(f32[16,1024]{1,0:T(8,128)S(1)} %collective-permute-done.3), channel_id=1, source_target_pairs={{0,2},{2,4},{4,6},{6,8},{8,10},{10,12},{12,14},{14,16},{16,18},{18... | collective-permute-start | bytes 196616 | tf_op jit(solution)/shard_map/ppermute | solution.py:19
  261.3 78.3 %copy-start.5 = (f32[16,1024]{1,0:T(8,128)}, f32[16,1024]{1,0:T(8,128)S(1)}, u32[]{:S(2)}) copy-start(f32[16,1024]{1,0:T(8,128)S(1)} %collective-permute-done.4) | copy-start | bytes 196612
  261.3 7.9 %collective-permute-start.5 = (f32[16,1024]{1,0:T(8,128)S(1)}, f32[16,1024]{1,0:T(8,128)S(1)}, u32[]{:S(2)}, u32[]{:S(2)}) collective-permute-start(f32[16,1024]{1,0:T(8,128)S(1)} %collective-permute-done.4), channel_id=1, source_target_pairs={{0,2},{2,4},{4,6},{6,8},{8,10},{10,12},{12,14},{14,16},{16,18},{18... | collective-permute-start | bytes 196616 | tf_op jit(solution)/shard_map/ppermute | solution.py:19
  269.2 0.6 copy-start.7
  269.8 7.9 %collective-permute-start.6 = (f32[16,1024]{1,0:T(8,128)S(1)}, f32[16,1024]{1,0:T(8,128)S(1)}, u32[]{:S(2)}, u32[]{:S(2)}) collective-permute-start(f32[16,1024]{1,0:T(8,128)S(1)} %collective-permute-done.5), channel_id=1, source_target_pairs={{0,2},{2,4},{4,6},{6,8},{8,10},{10,12},{12,14},{14,16},{16,18},{18... | collective-permute-start | bytes 196616 | tf_op jit(solution)/shard_map/ppermute | solution.py:19
  277.7 0.6 copy-start.9
  278.3 7.9 %collective-permute-start.7 = (f32[16,1024]{1,0:T(8,128)S(1)}, f32[16,1024]{1,0:T(8,128)S(1)}, u32[]{:S(2)}, u32[]{:S(2)}) collective-permute-start(f32[16,1024]{1,0:T(8,128)S(1)} %collective-permute-done.6), channel_id=1, source_target_pairs={{0,2},{2,4},{4,6},{6,8},{8,10},{10,12},{12,14},{14,16},{16,18},{18... | collective-permute-start | bytes 196616 | tf_op jit(solution)/shard_map/ppermute | solution.py:19
  286.2 0.6 copy-start.11
  286.8 7.9 %collective-permute-start.8 = (f32[16,1024]{1,0:T(8,128)S(1)}, f32[16,1024]{1,0:T(8,128)S(1)}, u32[]{:S(2)}, u32[]{:S(2)}) collective-permute-start(f32[16,1024]{1,0:T(8,128)S(1)} %collective-permute-done.7), channel_id=1, source_target_pairs={{0,2},{2,4},{4,6},{6,8},{8,10},{10,12},{12,14},{14,16},{16,18},{18... | collective-permute-start | bytes 196616 | tf_op jit(solution)/shard_map/ppermute | solution.py:19
  294.6 0.6 copy-start.13
  295.3 8.2 %collective-permute-start.9 = (f32[16,1024]{1,0:T(8,128)S(1)}, f32[16,1024]{1,0:T(8,128)S(1)}, u32[]{:S(2)}, u32[]{:S(2)}) collective-permute-start(f32[16,1024]{1,0:T(8,128)S(1)} %collective-permute-done.8), channel_id=1, source_target_pairs={{0,2},{2,4},{4,6},{6,8},{8,10},{10,12},{12,14},{14,16},{16,18},{18... | collective-permute-start | bytes 196616 | tf_op jit(solution)/shard_map/ppermute | solution.py:19
  303.5 0.6 copy-start.15
  304.1 7.9 %collective-permute-start.10 = (f32[16,1024]{1,0:T(8,128)S(1)}, f32[16,1024]{1,0:T(8,128)S(1)}, u32[]{:S(2)}, u32[]{:S(2)}) collective-permute-start(f32[16,1024]{1,0:T(8,128)S(1)} %collective-permute-done.9), channel_id=1, source_target_pairs={{0,2},{2,4},{4,6},{6,8},{8,10},{10,12},{12,14},{14,16},{16,18},{18... | collective-permute-start | bytes 196616 | tf_op jit(solution)/shard_map/ppermute | solution.py:19
  312.0 0.6 copy-start.17
  312.6 7.9 %collective-permute-start.11 = (f32[16,1024]{1,0:T(8,128)S(1)}, f32[16,1024]{1,0:T(8,128)S(1)}, u32[]{:S(2)}, u32[]{:S(2)}) collective-permute-start(f32[16,1024]{1,0:T(8,128)S(1)} %collective-permute-done.10), channel_id=1, source_target_pairs={{0,2},{2,4},{4,6},{6,8},{8,10},{10,12},{12,14},{14,16},{16,18},{18... | collective-permute-start | bytes 196616 | tf_op jit(solution)/shard_map/ppermute | solution.py:19
  320.5 0.6 copy-start.19
  321.1 7.9 %collective-permute-start.12 = (f32[16,1024]{1,0:T(8,128)S(1)}, f32[16,1024]{1,0:T(8,128)S(1)}, u32[]{:S(2)}, u32[]{:S(2)}) collective-permute-start(f32[16,1024]{1,0:T(8,128)S(1)} %collective-permute-done.11), channel_id=1, source_target_pairs={{0,2},{2,4},{4,6},{6,8},{8,10},{10,12},{12,14},{14,16},{16,18},{18... | collective-permute-start | bytes 196616 | tf_op jit(solution)/shard_map/ppermute | solution.py:19
  329.0 0.6 copy-start.21
  329.6 8.0 %collective-permute-start.13 = (f32[16,1024]{1,0:T(8,128)S(1)}, f32[16,1024]{1,0:T(8,128)}, u32[]{:S(2)}, u32[]{:S(2)}) collective-permute-start(f32[16,1024]{1,0:T(8,128)S(1)} %collective-permute-done.12), channel_id=1, source_target_pairs={{0,2},{2,4},{4,6},{6,8},{8,10},{10,12},{12,14},{14,16},{16,18},{18... | collective-permute-start | bytes 196616 | tf_op jit(solution)/shard_map/ppermute | solution.py:19
  337.6 8.2 %collective-permute-start.14 = (f32[16,1024]{1,0:T(8,128)}, f32[16,1024]{1,0:T(8,128)}, u32[]{:S(2)}, u32[]{:S(2)}) collective-permute-start(f32[16,1024]{1,0:T(8,128)} %collective-permute-done.13), channel_id=1, source_target_pairs={{0,2},{2,4},{4,6},{6,8},{8,10},{10,12},{12,14},{14,16},{16,18},{18... | collective-permute-start | bytes 196616 | tf_op jit(solution)/shard_map/ppermute | solution.py:19
  339.6 18.3 %copy-start.2 = (bf16[128,256]{1,0:T(8,128)(2,1)S(1)}, bf16[128,256]{1,0:T(8,128)(2,1)}, u32[]{:S(2)}) copy-start(bf16[128,256]{1,0:T(8,128)(2,1)} %param.17) | copy-start | bytes 196612
  339.6 191.2 %all-gather.12.cloned.1.call-start = ((), (), s32[]{:S(2)}) async-start(), calls=%async_computation.4 | async-start | bytes 4456448 | tf_op jit(solution)/shard_map/all_gather | solution.py:84
  339.7 17.1 %copy-start.22 = (f32[16,1024]{1,0:T(8,128)S(1)}, f32[16,1024]{1,0:T(8,128)}, u32[]{:S(2)}) copy-start(f32[16,1024]{1,0:T(8,128)} %copy-done.21) | copy-start | bytes 196612
  339.7 17.1 %copy-start.20 = (f32[16,1024]{1,0:T(8,128)S(1)}, f32[16,1024]{1,0:T(8,128)}, u32[]{:S(2)}) copy-start(f32[16,1024]{1,0:T(8,128)} %copy-done.19) | copy-start | bytes 196612
  339.7 17.1 %copy-start.18 = (f32[16,1024]{1,0:T(8,128)S(1)}, f32[16,1024]{1,0:T(8,128)}, u32[]{:S(2)}) copy-start(f32[16,1024]{1,0:T(8,128)} %copy-done.17) | copy-start | bytes 196612
  339.7 17.2 %copy-start.16 = (f32[16,1024]{1,0:T(8,128)S(1)}, f32[16,1024]{1,0:T(8,128)}, u32[]{:S(2)}) copy-start(f32[16,1024]{1,0:T(8,128)} %copy-done.15) | copy-start | bytes 196612
  339.7 17.2 %copy-start.14 = (f32[16,1024]{1,0:T(8,128)S(1)}, f32[16,1024]{1,0:T(8,128)}, u32[]{:S(2)}) copy-start(f32[16,1024]{1,0:T(8,128)} %copy-done.13) | copy-start | bytes 196612
  339.7 17.2 %copy-start.12 = (f32[16,1024]{1,0:T(8,128)S(1)}, f32[16,1024]{1,0:T(8,128)}, u32[]{:S(2)}) copy-start(f32[16,1024]{1,0:T(8,128)} %copy-done.11) | copy-start | bytes 196612
  339.8 17.2 %copy-start.10 = (f32[16,1024]{1,0:T(8,128)S(1)}, f32[16,1024]{1,0:T(8,128)}, u32[]{:S(2)}) copy-start(f32[16,1024]{1,0:T(8,128)} %copy-done.9) | copy-start | bytes 196612
  339.8 17.2 %copy-start.8 = (f32[16,1024]{1,0:T(8,128)S(1)}, f32[16,1024]{1,0:T(8,128)}, u32[]{:S(2)}) copy-start(f32[16,1024]{1,0:T(8,128)} %copy-done.7) | copy-start | bytes 196612
  339.8 17.2 %copy-start.6 = (f32[16,1024]{1,0:T(8,128)S(1)}, f32[16,1024]{1,0:T(8,128)}, u32[]{:S(2)}) copy-start(f32[16,1024]{1,0:T(8,128)} %copy-done.5) | copy-start | bytes 196612
  355.1 41.2 %copy-start.3 = (bf16[128,256]{1,0:T(8,128)(2,1)S(1)}, bf16[128,256]{1,0:T(8,128)(2,1)}, u32[]{:S(2)}) copy-start(bf16[128,256]{1,0:T(8,128)(2,1)} %param.16) | copy-start | bytes 196612
  441.4 179.0 %all-gather.14.cloned.1.call-start = ((), (), s32[]{:S(2)}) async-start(), calls=%async_computation.5 | async-start | bytes 4456448 | tf_op jit(solution)/shard_map/all_gather | solution.py:85
Sparse Core Ops, SparseCore 0:
  10.7 57.7 all-gather.5
  71.3 53.9 all-gather.7
  139.3 80.4 reduce-scatter.3
  339.7 56.4 all-gather.9
  441.5 89.3 all-gather.11
  533.4 86.8 all-gather.13
